TPU v7x, 32 devices: a whole 2x2x4 slice. The times are simulated.
32 devices in a mesh: ep: 4 (over y, x), tp: 8 (over z, core).
Axes of the slice: x: 2, y: 2, z: 4, core: 2. Of those that a mesh axis runs over, the one named last changes fastest.
Arguments:
- queries: bfloat16 [3072, 2048], P('ep', 'tp'), may hold values from -6 to 6
- keys: bfloat16 [3072, 512], P('ep'), may hold values from -6 to 6
- values: bfloat16 [3072, 512], P('ep'), may hold values from -6 to 6
- query_gain: float32 [128], replicated, may hold values from 1 to 4.5
- key_gain: float32 [128], replicated, may hold values from 1 to 4.5
- out_weight: bfloat16 [2048, 2048], P('tp'), may hold values from -0.75 to 0.75
- tokens_b: bfloat16 [1536, 2048], P('ep'), may hold values from -6 to 6
- norm_gain: float32 [2048], replicated, may hold values from 0.1 to 1.9
- routes: int32 [1536, 2], P('ep'), may hold values from 0 to 15, all different within a row; in each aligned block of 48 rows (0 to 47, 48 to 95, ...) at most 8 rows name the same one
- route_weight: float32 [1536, 2], P('ep'), may hold values from 0.2 to 1
- gate_weight: bfloat16 [16, 2048, 4096], P('ep', None, 'tp'), may hold values from -0.125 to 0.125
- up_weight: bfloat16 [16, 2048, 4096], P('ep', None, 'tp'), may hold values from -0.125 to 0.125
- down_weight: bfloat16 [16, 4096, 2048], P('ep', 'tp'), may hold values from -0.09375 to 0.09375
Outputs:
- mixed_out: bfloat16 [3072, 2048], P(('ep', 'tp'))
- expert_out: bfloat16 [1536, 2048], P(('ep', 'tp'))
Inputs may be any that keep to these rules, and one draw needn't show every extreme that they name: `routes`: A row names 2 different experts. In each aligned block of 48 rows no expert is named more than 8 times, a bound that some block reaches.
All inputs are finite; a program needn't handle non-finite values.
Results may differ from a plain program's by a relative error of at most 0.019.
Values may be sent and summed in bfloat16 or wider, within the bound.
No kernel may reach another device: no remote copies, remote signals or barrier semaphores. Data moves between devices by JAX's collectives and lax.ppermute only.
A program may use at most 128 MiB of HBM per device.

v0:
```python
import jax
import jax.numpy as jnp
from jax import lax
from jax.sharding import PartitionSpec as P

D = 2048
HD = 128
HQ = 16
KVH = 4
EXPERTS = 16
TOPK = 2
GRID_W = 64
CAP = 8
EPS = 1e-06
THETA = 10000.0


def rotate(field, positions):
    n_freq = HD // 4
    row_pos = (positions // GRID_W).astype(jnp.float32)
    col_pos = (positions % GRID_W).astype(jnp.float32)
    inverse = THETA ** (-jnp.arange(n_freq, dtype=jnp.float32) / n_freq)
    angles = jnp.stack([row_pos[:, None] * inverse, col_pos[:, None] * inverse], axis=1)
    cosine = jnp.cos(angles)[:, None]
    sine = jnp.sin(angles)[:, None]
    length, n_heads = (field.shape[0], field.shape[1])
    halves = field.reshape(length, n_heads, 2, 2, n_freq)
    leading = halves[..., 0, :]
    second = halves[..., 1, :]
    turned = jnp.stack(
        [leading * cosine - second * sine, second * cosine + leading * sine], axis=-2
    )
    return turned.reshape(length, n_heads, HD)


def prepare(source, gain_vec, positions, n_heads):
    length = source.shape[0]
    field = source.astype(jnp.float32).reshape(length, n_heads, HD)
    field = field * lax.rsqrt(jnp.mean(field * field, axis=-1, keepdims=True) + EPS) * gain_vec
    return rotate(field, positions).astype(jnp.bfloat16)


def token_mixer(queries, keys, values, query_gain, key_gain, out_weight):
    n_rows = queries.shape[0]
    q_heads = queries.shape[1] // HD
    positions = lax.axis_index("ep") * n_rows + jnp.arange(n_rows, dtype=jnp.int32)
    query_n = prepare(queries, query_gain, positions, q_heads).reshape(n_rows * q_heads, HD)
    kv_index = lax.axis_index("tp") * q_heads // (HQ // KVH)
    own_keys = prepare(
        lax.dynamic_slice_in_dim(keys, kv_index * HD, HD, 1), key_gain, positions, 1
    ).reshape(n_rows, HD)
    own_values = lax.dynamic_slice_in_dim(values, kv_index * HD, HD, 1)
    score_scale = HD ** (-0.5)
    start_state = (
        jnp.full((n_rows * q_heads,), -1e30, jnp.float32),
        jnp.zeros((n_rows * q_heads,), jnp.float32),
        jnp.zeros((n_rows * q_heads, HD), jnp.float32),
    )
    key_piece = lax.all_gather(own_keys, "ep", axis=0, tiled=True)
    value_piece = lax.all_gather(own_values, "ep", axis=0, tiled=True)
    steps_n = key_piece.shape[0] // n_rows

    def one_block(index_b, state):
        running_max, totals, numerator = state
        key_blk = lax.dynamic_slice_in_dim(key_piece, index_b * n_rows, n_rows, 0)
        value_blk = lax.dynamic_slice_in_dim(value_piece, index_b * n_rows, n_rows, 0)
        scores = (
            jnp.einsum("qd,sd->qs", query_n, key_blk, preferred_element_type=jnp.float32)
            * score_scale
        )
        new_max = jnp.maximum(running_max, jnp.max(scores, axis=1))
        shrink = jnp.exp(running_max - new_max)
        weights = jnp.exp(scores - new_max[:, None])
        totals = totals * shrink + jnp.sum(weights, axis=1)
        numerator = numerator * shrink[:, None] + jnp.dot(
            weights.astype(jnp.bfloat16), value_blk, preferred_element_type=jnp.float32
        )
        return (new_max, totals, numerator)

    running_max, totals, numerator = lax.fori_loop(0, steps_n, one_block, start_state)
    attended = (numerator / totals[:, None]).astype(jnp.bfloat16).reshape(n_rows, q_heads * HD)
    return lax.psum_scatter(
        jnp.dot(attended, out_weight, preferred_element_type=jnp.float32).astype(jnp.bfloat16),
        "tp",
        scatter_dimension=0,
        tiled=True,
    )


def expert_half(tokens_b, norm_gain, routes, route_weight, gate_weight, up_weight, down_weight):
    n_tp = lax.axis_size("tp")
    n_ep = lax.axis_size("ep")
    tp_index = lax.axis_index("tp")
    local_rows = tokens_b.shape[0]
    block_rows = local_rows // n_tp
    picks = block_rows * TOPK
    local_experts = gate_weight.shape[0]
    assigned = routes.reshape(n_tp, picks)
    onehot = (assigned[:, :, None] == jnp.arange(EXPERTS, dtype=jnp.int32)[None, None, :]).astype(
        jnp.int32
    )
    slot_rank = jnp.sum((jnp.cumsum(onehot, axis=1) - onehot) * onehot, axis=-1)
    target = assigned * CAP + slot_rank
    target_hot = (
        target[:, :, None] == jnp.arange(EXPERTS * CAP, dtype=jnp.int32)[None, None, :]
    ).astype(jnp.float32)
    token_hot = (
        jnp.arange(picks, dtype=jnp.int32)[:, None] // TOPK
        == jnp.arange(block_rows, dtype=jnp.int32)[None, :]
    ).astype(jnp.float32)
    field = tokens_b.astype(jnp.float32)
    normed = (
        field * lax.rsqrt(jnp.mean(field * field, axis=-1, keepdims=True) + EPS) * norm_gain
    ).astype(jnp.bfloat16)
    dispatch_mat = jnp.einsum(
        "baj,at->bjt", target_hot, token_hot, precision=lax.Precision.HIGHEST
    ).astype(jnp.bfloat16)
    outgoing = jnp.einsum(
        "bjt,btd->bjd",
        dispatch_mat,
        normed.reshape(n_tp, block_rows, D),
        preferred_element_type=jnp.float32,
    )
    outgoing = outgoing.astype(jnp.bfloat16).reshape(n_tp, EXPERTS, CAP, D)
    arrived = lax.all_to_all(outgoing, "ep", split_axis=1, concat_axis=2, tiled=True)
    flat_rows = arrived.reshape(-1, D)
    share_rows = flat_rows.shape[0] // n_tp
    expert_slab_rows = flat_rows.reshape(
        share_rows * lax.axis_size("tp") // share_rows, local_experts, n_ep * CAP, D
    )
    gate_act = jnp.einsum(
        "blmd,ldf->blmf", expert_slab_rows, gate_weight, preferred_element_type=jnp.float32
    )
    up_act = jnp.einsum(
        "blmd,ldf->blmf", expert_slab_rows, up_weight, preferred_element_type=jnp.float32
    )
    hidden = (jax.nn.silu(gate_act) * up_act).astype(jnp.bfloat16)
    result = jnp.einsum("blmf,lfd->blmd", hidden, down_weight, preferred_element_type=jnp.float32)
    summed = lax.psum_scatter(
        result.reshape(-1, D).astype(jnp.bfloat16), "tp", scatter_dimension=0, tiled=True
    )
    returned = lax.all_to_all(
        summed.reshape(local_experts, n_ep, CAP, D), "ep", split_axis=1, concat_axis=0, tiled=True
    )
    returned = returned.reshape(EXPERTS * CAP, D)
    own_target = lax.dynamic_index_in_dim(target_hot, tp_index, 0, keepdims=False)
    shares = (route_weight / jnp.sum(route_weight, axis=-1, keepdims=True)).reshape(n_tp, picks)
    own_shares = lax.dynamic_index_in_dim(shares, tp_index, 0, keepdims=False)
    combine = jnp.einsum(
        "at,aj->tj", token_hot, own_target * own_shares[:, None], precision=lax.Precision.HIGHEST
    )
    return jnp.dot(combine, returned.astype(jnp.float32), precision=lax.Precision.HIGHEST).astype(
        jnp.bfloat16
    )


def on_device(
    queries,
    keys,
    values,
    query_gain,
    key_gain,
    out_weight,
    tokens_b,
    norm_gain,
    routes,
    route_weight,
    gate_weight,
    up_weight,
    down_weight,
):
    mixed_out = token_mixer(queries, keys, values, query_gain, key_gain, out_weight)
    expert_out = expert_half(
        tokens_b, norm_gain, routes, route_weight, gate_weight, up_weight, down_weight
    )
    return (mixed_out, expert_out)


def solution(mesh):
    placed = (
        P("ep", "tp"),
        P("ep", None),
        P("ep", None),
        P(),
        P(),
        P("tp", None),
        P("ep", None),
        P(),
        P("ep", None),
        P("ep", None),
        P("ep", None, "tp"),
        P("ep", None, "tp"),
        P("ep", "tp", None),
    )
    return jax.shard_map(
        on_device,
        mesh=mesh,
        in_specs=placed,
        out_specs=(P(("ep", "tp"), None), P(("ep", "tp"), None)),
        check_vma=False,
    )
```

profile of v0, /device:TPU:0, one launch (start us, length us, event | category | flops | bytes accessed | tf_op | source)
XLA Modules:
  0.0 199.7 jit_solution(16089087401707294677)
XLA Ops:
  7.2 1.9 fusion.24
  9.1 0.8 copy.47
  9.9 0.1 reshape.432
  10.1 1.9 select_reduce_fusion
  12.1 0.3 convolution_convert_fusion.2
  12.5 1.8 fusion.26
  14.3 1.3 convert_bitcast_fusion.1
  15.6 2.3 %copy.51 = bf16[8,16,8,2048]{3,2,0,1:T(8,128)(2,1)} copy(bf16[8,16,8,2048]{3,2,1,0:T(8,128)(2,1)S(1)} %convert_bitcast_fusion.1) | data formatting | bytes 8388608 | tf_op jit(solution)/shard_map/reshape | solution.py:124
  17.9 5.3 %all-to-all-start = ((bf16[8,16,8,2048]{3,2,0,1:T(8,128)(2,1)}), bf16[8,16,8,2048]{3,2,0,1:T(8,128)(2,1)}, u32[]{:S(2)}, u32[]{:S(2)}) async-start(bf16[8,16,8,2048]{3,2,0,1:T(8,128)(2,1)} %copy.51), calls=%async_computation.1 | async-start | bytes 8388608 | tf_op jit(solution)/shard_map/all_to_all | solution.py:125
  23.3 0.2 copy.44
  23.6 0.7 fusion.48
  24.7 47.1 %all-to-all-done = bf16[8,16,8,2048]{3,2,0,1:T(8,128)(2,1)} async-done(((bf16[8,16,8,2048]{3,2,0,1:T(8,128)(2,1)}), bf16[8,16,8,2048]{3,2,0,1:T(8,128)(2,1)}, u32[]{:S(2)}, u32[]{:S(2)}) %all-to-all-start) | async-done | bytes 4194336 | tf_op jit(solution)/shard_map/all_to_all | solution.py:125
  71.8 8.4 %fusion.16 = f32[4,8,32,512]{3,2,1,0:T(8,128)} fusion(bf16[4,2048,512]{2,1,0:T(8,128)(2,1)} %param.25, bf16[8,4,4,8,2048]{4,3,0,2,1:T(8,128)(2,1)} %bitcast.11), kind=kOutput, calls=%fused_computation.22 | convolution fusion | flops 2147483648 | bytes 14680064 | tf_op jit(solution)/shard_map/blmd,ldf->blmf/dot_general | solution.py:131
  80.2 14.2 %convert_bitcast_fusion = bf16[8,4,32,2048]{3,2,0,1:T(8,128)(2,1)} fusion(bf16[4,512,2048]{2,1,0:T(8,128)(2,1)} %param.27, f32[4,8,32,512]{3,2,1,0:T(8,128)} %fusion.16, bf16[4,2048,512]{2,1,0:T(8,128)(2,1)} %param.26, bf16[8,4,4,8,2048]{4,3,0,2,1:T(8,128)(2,1)} %bitcast.11), kind=kOutput, calls=%fused_computation.26 | convolution fusion | flops 4300210176 | bytes 27262976 | tf_op jit(solution)/shard_map/blmf,lfd->blmd/dot_general | solution.py:138
  94.4 4.7 %copy.53 = bf16[8,4,32,2048]{3,2,1,0:T(8,128)(2,1)} copy(bf16[8,4,32,2048]{3,2,0,1:T(8,128)(2,1)} %convert_bitcast_fusion) | data formatting | bytes 8388608 | tf_op jit(solution)/shard_map/convert_element_type | solution.py:140
  99.1 0.2 reduce-scatter.3.cloned.1.call-start
  99.3 0.9 constant_dynamic-slice_fusion.2
  100.3 0.1 copy.59
  100.5 2.9 %copy.45 = bf16[768,2,2,2,32]{4,3,2,1,0:T(2,128)(2,1)} copy(bf16[768,2,2,2,32]{0,4,3,2,1:T(8,128)(2,1)S(1)} %pad_maximum_fusion) | data formatting | bytes 786432 | tf_op jit(solution)/shard_map/stack | solution.py:30
  103.4 3.7 %convert_element_type.88 = bf16[1536,128]{1,0:T(8,128)(2,1)S(1)} reshape(bf16[768,2,2,2,32]{4,3,2,1,0:T(2,128)(2,1)} %copy.45) | data formatting | bytes 786432 | tf_op jit(solution)/shard_map/convert_element_type | solution.py:40
  107.1 0.9 constant_dynamic-slice_fusion.1
  108.2 0.7 subtract_convert_fusion.1
  109.0 12.7 %all_gather.6 = bf16[3072,128]{0,1:T(8,128)(2,1)S(1)} all-gather(bf16[768,128]{0,1:T(8,128)(2,1)S(1)} %bitcast.98), channel_id=1, replica_groups=mesh['ep'=4,'tp'=8] {'ep'}, dimensions={0}, use_global_device_ids=true | all-gather | bytes 983040 | tf_op jit(solution)/shard_map/all_gather | solution.py:59
  121.7 11.2 %all_gather.7 = bf16[3072,128]{1,0:T(8,128)(2,1)} all-gather(bf16[768,128]{1,0:T(8,128)(2,1)S(1)} %constant_dynamic-slice_fusion.1), channel_id=1, replica_groups=mesh['ep'=4,'tp'=8] {'ep'}, dimensions={0}, use_global_device_ids=true | all-gather | bytes 983040 | tf_op jit(solution)/shard_map/all_gather | solution.py:60
  132.9 15.4 %while.18 = (s32[]{:T(128)}, f32[1536]{0:T(1024)S(1)}, f32[1536]{0:T(1024)S(1)}, f32[1536,128]{1,0:T(8,128)S(1)}, bf16[3072,128]{0,1:T(8,128)(2,1)S(1)}, /*index...) while((s32[]{:T(128)}, f32[1536]{0:T(1024)S(1)}, ...), condition=%wide.region_5.6_spmd.clone, body=%wide.region_2.5_spmd.clone.sunk | while | flops 614014464 | bytes 16613559 | solution.py:80
  132.9 0.8 multiply_reduce_fusion.2
  133.8 0.8 fusion.86
  134.6 2.1 %convolution_add_fusion.2 = f32[1536,128]{1,0:T(8,128)S(1)} fusion(f32[768,1536]{1,0:T(8,128)S(1)} %get-tuple-element.254, f32[1536]{0:T(1024)S(1)} %select_maximum_fusion.2, f32[1536,128]{1,0:T(8,128)S(1)} %get-tuple-element.271, f32[1536]{0:T(1024)S(1)} %get-tuple-element.256, pred[]{:T(512)S(6)} %compare.22, ...), kind=kOutput, calls=%fused_computation.4.clone.1 | convolution fusion | flops 306118656 | bytes 6500357 | tf_op jit(solution)/shard_map/while/body/eval_jaxpr/dot_general | solution.py:75
  136.8 0.8 multiply_reduce_fusion.2
  137.6 0.8 fusion.86
  138.4 2.1 %convolution_add_fusion.2 = f32[1536,128]{1,0:T(8,128)S(1)} fusion(f32[768,1536]{1,0:T(8,128)S(1)} %get-tuple-element.254, f32[1536]{0:T(1024)S(1)} %select_maximum_fusion.2, f32[1536,128]{1,0:T(8,128)S(1)} %get-tuple-element.271, f32[1536]{0:T(1024)S(1)} %get-tuple-element.256, pred[]{:T(512)S(6)} %compare.22, ...), kind=kOutput, calls=%fused_computation.4.clone.1 | convolution fusion | flops 306118656 | bytes 6500357 | tf_op jit(solution)/shard_map/while/body/eval_jaxpr/dot_general | solution.py:75
  140.6 0.8 multiply_reduce_fusion.2
  141.5 0.8 fusion.86
  142.3 2.2 %convolution_add_fusion.2 = f32[1536,128]{1,0:T(8,128)S(1)} fusion(f32[768,1536]{1,0:T(8,128)S(1)} %get-tuple-element.254, f32[1536]{0:T(1024)S(1)} %select_maximum_fusion.2, f32[1536,128]{1,0:T(8,128)S(1)} %get-tuple-element.271, f32[1536]{0:T(1024)S(1)} %get-tuple-element.256, pred[]{:T(512)S(6)} %compare.22, ...), kind=kOutput, calls=%fused_computation.4.clone.1 | convolution fusion | flops 306118656 | bytes 6500357 | tf_op jit(solution)/shard_map/while/body/eval_jaxpr/dot_general | solution.py:75
  144.5 0.8 multiply_reduce_fusion.2
  145.3 0.8 fusion.86
  146.1 2.2 %convolution_add_fusion.2 = f32[1536,128]{1,0:T(8,128)S(1)} fusion(f32[768,1536]{1,0:T(8,128)S(1)} %get-tuple-element.254, f32[1536]{0:T(1024)S(1)} %select_maximum_fusion.2, f32[1536,128]{1,0:T(8,128)S(1)} %get-tuple-element.271, f32[1536]{0:T(1024)S(1)} %get-tuple-element.256, pred[]{:T(512)S(6)} %compare.22, ...), kind=kOutput, calls=%fused_computation.4.clone.1 | convolution fusion | flops 306118656 | bytes 6500357 | tf_op jit(solution)/shard_map/while/body/eval_jaxpr/dot_general | solution.py:75
  148.3 0.3 divide_convert_fusion
  148.8 2.7 %convolution_convert_fusion = bf16[768,2048]{1,0:T(8,128)(2,1)} fusion(bf16[768,256]{1,0:T(8,128)(2,1)S(1)} %reshape.431, bf16[256,2048]{1,0:T(8,128)(2,1)S(1)} %copy-done), kind=kOutput, calls=%fused_computation.32 | convolution fusion | flops 806879232 | bytes 4587520 | tf_op jit(solution)/shard_map/dot_general | solution.py:83
  151.5 0.2 iota_compare_fusion
  151.7 1.9 copy.54
  153.6 3.5 %all-to-all-start.1 = ((bf16[4,4,8,2048]{3,2,0,1:T(8,128)(2,1)}), bf16[4,4,8,2048]{3,2,0,1:T(8,128)(2,1)S(1)}, u32[]{:S(2)}, u32[]{:S(2)}) async-start(bf16[4,4,8,2048]{3,2,0,1:T(8,128)(2,1)} %copy.54), calls=%async_computation.3 | async-start | bytes 1048576 | tf_op jit(solution)/shard_map/all_to_all | solution.py:142
  157.1 0.1 copy.50
  157.2 0.1 reshape.433
  157.4 0.2 fusion.51
  157.6 6.0 %all-to-all-done.1 = bf16[4,4,8,2048]{3,2,0,1:T(8,128)(2,1)S(1)} async-done(((bf16[4,4,8,2048]{3,2,0,1:T(8,128)(2,1)}), bf16[4,4,8,2048]{3,2,0,1:T(8,128)(2,1)S(1)}, u32[]{:S(2)}, u32[]{:S(2)}) %all-to-all-start.1) | async-done | bytes 524320 | tf_op jit(solution)/shard_map/all_to_all | solution.py:142
  163.6 1.0 convolution_convert_fusion.1
  164.6 28.2 %reduce-scatter.3.cloned.1.call-done = bf16[96,2048]{1,0:T(8,128)(2,1)} async-done(((bf16[768,2048]{1,0:T(8,128)(2,1)}), bf16[96,2048]{1,0:T(8,128)(2,1)}) %reduce-scatter.3.cloned.1.call-update) | async-done | bytes 393232 | tf_op jit(solution)/shard_map/reduce_scatter | solution.py:82
  (51 shorter events, 1.3 us)
Async XLA Ops:
  7.2 141.6 %copy-start = (bf16[256,2048]{1,0:T(8,128)(2,1)S(1)}, bf16[256,2048]{1,0:T(8,128)(2,1)}, u32[]{:S(2)}) copy-start(bf16[256,2048]{1,0:T(8,128)(2,1)} %param.20) | copy-start | bytes 3145732
  17.9 5.3 %copy-start.3 = (f32[128]{0:T(128)S(1)}, f32[128]{0:T(128)}, u32[]{:S(2)}) copy-start(f32[128]{0:T(128)} %param.18) | copy-start | bytes 1540
  17.9 5.4 %copy-start.1 = (bf16[768,256]{1,0:T(8,128)(2,1)S(1)}, bf16[768,256]{1,0:T(8,128)(2,1)}, u32[]{:S(2)}) copy-start(bf16[768,256]{1,0:T(8,128)(2,1)} %param.15) | copy-start | bytes 1179652
  17.9 53.9 %all-to-all-start = ((bf16[8,16,8,2048]{3,2,0,1:T(8,128)(2,1)}), bf16[8,16,8,2048]{3,2,0,1:T(8,128)(2,1)}, u32[]{:S(2)}, u32[]{:S(2)}) async-start(bf16[8,16,8,2048]{3,2,0,1:T(8,128)(2,1)} %copy.51), calls=%async_computation.1 | async-start | bytes 8388608 | tf_op jit(solution)/shard_map/all_to_all | solution.py:125
  23.2 128.5 %reduce-scatter.5.cloned.1.call-start = ((), (), s32[]{:S(2)}) async-start(), calls=%async_computation.5 | async-start | bytes 4718592 | tf_op jit(solution)/shard_map/reduce_scatter | solution.py:139
  99.1 9.0 %copy-start.4 = (f32[128]{0:T(128)S(1)}, f32[128]{0:T(128)}, u32[]{:S(2)}) copy-start(f32[128]{0:T(128)} %param.19) | copy-start | bytes 1540
  99.1 93.7 %reduce-scatter.3.cloned.1.call-start = ((), (), s32[]{:S(2)}) async-start(), calls=%async_computation.4 | async-start | bytes 3538944 | tf_op jit(solution)/shard_map/reduce_scatter | solution.py:82
  148.7 2.7 %copy-start.2 = (f32[384,2]{0,1:T(2,128)S(1)}, f32[384,2]{0,1:T(2,128)}, u32[]{:S(2)}) copy-start(f32[384,2]{0,1:T(2,128)} %param.24) | copy-start | bytes 9220
  153.6 10.0 %all-to-all-start.1 = ((bf16[4,4,8,2048]{3,2,0,1:T(8,128)(2,1)}), bf16[4,4,8,2048]{3,2,0,1:T(8,128)(2,1)S(1)}, u32[]{:S(2)}, u32[]{:S(2)}) async-start(bf16[4,4,8,2048]{3,2,0,1:T(8,128)(2,1)} %copy.54), calls=%async_computation.3 | async-start | bytes 1048576 | tf_op jit(solution)/shard_map/all_to_all | solution.py:142
Sparse Core Ops, SparseCore 0:
  99.2 50.3 reduce-scatter.4
  152.6 40.2 reduce-scatter.2
where the time goes:
time: 200 us
  waiting for transfers between devices  81.4 us (41%)
  matrix products  40 us (20%)
  blocking collectives  23.9 us (12%)
  local copies, waits for them, and re-layouts  19.3 us (10%)
  between operations  14.3 us (7%)
  other arithmetic  11.5 us (6%)
  starting transfers between devices  9.02 us (5%)
    all_to_all x1, waiting for transfers between devices, expert_half(): lax.all_to_all(outgoing, 'ep', split_axis=1, concat_axis=2, tiled=True)  47.1 us
    reduce_scatter x1, waiting for transfers between devices, token_mixer(): lax.psum_scatter(jnp.dot(attended, out_weight, preferred_element_type=jnp...  28.2 us
    dot_general x1, matrix products, expert_half(): jnp.einsum('blmf,lfd->blmd', hidden, down_weight, preferred_element_type=...  14.2 us
    all_gather x1, blocking collectives, token_mixer(): key_piece = lax.all_gather(own_keys, 'ep', axis=0, tiled=True)  12.7 us
    all_gather x1, blocking collectives, token_mixer(): value_piece = lax.all_gather(own_values, 'ep', axis=0, tiled=True)  11.2 us
    dot_general x4, matrix products, one_block(): jnp.dot(weights.astype(jnp.bfloat16), value_blk, preferred_element_type=j...  8.6 us
    dot_general x1, matrix products, expert_half(): jnp.einsum('blmd,ldf->blmf', expert_slab_rows, gate_weight, preferred_ele...  8.38 us
    all_to_all x1, waiting for transfers between devices, expert_half(): lax.all_to_all(summed.reshape(local_experts, n_ep, CAP, D), 'ep', split_a...  6.01 us
  transfers between devices with their start and end apart: 4, of which 3 were waited for; matrix products, arithmetic and copies ran while one was open for 16% of the time, Pallas kernels for 0%

commit v1 on v0

--- a/solution.py
+++ b/solution.py
@@ -122,7 +122,10 @@
         preferred_element_type=jnp.float32,
     )
     outgoing = outgoing.astype(jnp.bfloat16).reshape(n_tp, EXPERTS, CAP, D)
-    arrived = lax.all_to_all(outgoing, "ep", split_axis=1, concat_axis=2, tiled=True)
+    arrived = jnp.concatenate(
+        lax.all_to_all(jnp.stack(jnp.split(outgoing, lax.axis_size("ep"), axis=1)), "ep", 0, 0),
+        axis=2,
+    )
     flat_rows = arrived.reshape(-1, D)
     share_rows = flat_rows.shape[0] // n_tp
     expert_slab_rows = flat_rows.reshape(

time: 200 us -> 221 us (1.10)
  other arithmetic: 11.5 us -> 23.7 us
  matrix products: 40 us -> 48.6 us
    reduce_sum x4, other arithmetic: 3.21 us -> 13.3 us  [one_block(): totals = totals * shrink + jnp.sum(weights, axis=1)]
    dot_general x4, matrix products: 3.31 us -> 12 us  [one_block(): jnp.einsum('qd,sd->qs', query_n, key_blk, preferred_element_type=jnp.floa...]
    reshape x1 -> x0, local copies, waits for them, and re-layouts: 2.28 us -> none  [expert_half(): outgoing = outgoing.astype(jnp.bfloat16).reshape(n_tp, EXPERTS, CAP, D)]
    another operation x2 -> x3, other arithmetic: 0.83 us -> 3.07 us  [the longest x1 2.25 us: expert_half(): jnp.stack(jnp.split(outgoing, lax.axis_size('ep'), axis=1))]
  transfers between devices with their start and end apart: 4 -> 4, of which waited for: 3 -> 3; matrix products, arithmetic and copies ran while one was open for 16% -> 23% of each run, Pallas kernels for 0% -> 0%
where the time goes in v1:
time: 221 us
  waiting for transfers between devices  81.3 us (37%)
  matrix products  48.6 us (22%)
  blocking collectives  24.2 us (11%)
  other arithmetic  23.7 us (11%)
  local copies, waits for them, and re-layouts  19.6 us (9%)
  between operations  14.3 us (6%)
  starting transfers between devices  8.84 us (4%)
    all_to_all x1, waiting for transfers between devices, expert_half(): lax.all_to_all(jnp.stack(jnp.split(outgoing, lax.axis_size('ep'), axis=1)...  47.1 us
    reduce_scatter x1, waiting for transfers between devices, token_mixer(): lax.psum_scatter(jnp.dot(attended, out_weight, preferred_element_type=jnp...  28.1 us
    dot_general x1, matrix products, expert_half(): jnp.einsum('blmf,lfd->blmd', hidden, down_weight, preferred_element_type=...  14.2 us
    reduce_sum x4, other arithmetic, one_block(): totals = totals * shrink + jnp.sum(weights, axis=1)  13.3 us
    all_gather x1, blocking collectives, token_mixer(): key_piece = lax.all_gather(own_keys, 'ep', axis=0, tiled=True)  12.7 us
    dot_general x4, matrix products, one_block(): jnp.einsum('qd,sd->qs', query_n, key_blk, preferred_element_type=jnp.floa...  12 us
    all_gather x1, blocking collectives, token_mixer(): value_piece = lax.all_gather(own_values, 'ep', axis=0, tiled=True)  11.4 us
    dot_general x4, matrix products, one_block(): jnp.dot(weights.astype(jnp.bfloat16), value_blk, preferred_element_type=j...  8.58 us
  transfers between devices with their start and end apart: 4, of which 3 were waited for; matrix products, arithmetic and copies ran while one was open for 23% of the time, Pallas kernels for 0%

profile of v1, /device:TPU:0, one launch (start us, length us, event | category | flops | bytes accessed | tf_op | source)
XLA Modules:
  0.0 220.7 jit_solution(18117744069012055431)
XLA Ops:
  7.2 0.9 copy.46
  8.3 1.9 select_reduce_fusion
  10.3 1.8 fusion.24
  12.1 0.3 convolution_convert_fusion.2
  12.4 1.8 fusion.26
  14.3 1.3 convert_bitcast_fusion.1
  15.6 0.6 slice_bitcast_fusion.3
  16.2 2.2 %pad_maximum_fusion = bf16[4,8,4,8,2048]{4,3,2,1,0:T(8,128)(2,1)} fusion(bf16[1,8,4,8,2048]{4,3,2,1,0:T(8,128)(2,1)S(1)} %get-tuple-element.193, bf16[1,8,4,8,2048]{4,3,2,1,0:T(8,128)(2,1)S(1)} %get-tuple-element.194, bf16[1,8,4,8,2048]{4,3,2,1,0:T(8,128)(2,1)S(1)} %get-tuple-element.195, bf16[1,8,4,8,2048]{4,3,2,1,0:T(8,128)(2,1)S(1)} %get-tuple-element.192), kind=kLoop, calls=%fused_computation.24 | loop fusion | flops 6291456 | bytes 8388608 | tf_op jit(solution)/shard_map/stack | solution.py:126
  18.4 5.3 %all-to-all-start = ((bf16[4,8,4,8,2048]{4,3,2,1,0:T(8,128)(2,1)}), bf16[4,8,4,8,2048]{4,3,2,1,0:T(8,128)(2,1)}, u32[]{:S(2)}, u32[]{:S(2)}) async-start(bf16[4,8,4,8,2048]{4,3,2,1,0:T(8,128)(2,1)} %pad_maximum_fusion), calls=%async_computation.1 | async-start | bytes 8388608 | tf_op jit(solution)/shard_map/all_to_all | solution.py:126
  23.7 0.2 copy.43
  24.2 0.7 fusion.48
  25.2 47.1 %all-to-all-done = bf16[4,8,4,8,2048]{4,3,2,1,0:T(8,128)(2,1)} async-done(((bf16[4,8,4,8,2048]{4,3,2,1,0:T(8,128)(2,1)}), bf16[4,8,4,8,2048]{4,3,2,1,0:T(8,128)(2,1)}, u32[]{:S(2)}, u32[]{:S(2)}) %all-to-all-start) | async-done | bytes 4194336 | tf_op jit(solution)/shard_map/all_to_all | solution.py:126
  72.4 8.4 %fusion.16 = f32[4,8,32,512]{3,2,1,0:T(8,128)} fusion(bf16[4,2048,512]{2,1,0:T(8,128)(2,1)} %param.25, bf16[4,8,4,8,2048]{4,3,2,1,0:T(8,128)(2,1)} %all-to-all-done), kind=kOutput, calls=%fused_computation.22 | convolution fusion | flops 2147483648 | bytes 14680064 | tf_op jit(solution)/shard_map/blmd,ldf->blmf/dot_general | solution.py:134
  80.7 14.2 %convert_bitcast_fusion = bf16[8,4,32,2048]{3,2,0,1:T(8,128)(2,1)} fusion(bf16[4,512,2048]{2,1,0:T(8,128)(2,1)} %param.27, f32[4,8,32,512]{3,2,1,0:T(8,128)} %fusion.16, bf16[4,2048,512]{2,1,0:T(8,128)(2,1)} %param.26, bf16[4,8,4,8,2048]{4,3,2,1,0:T(8,128)(2,1)} %all-to-all-done), kind=kOutput, calls=%fused_computation.27 | convolution fusion | flops 4300210176 | bytes 27262976 | tf_op jit(solution)/shard_map/blmf,lfd->blmd/dot_general | solution.py:141
  94.9 4.7 %copy.51 = bf16[8,4,32,2048]{3,2,1,0:T(8,128)(2,1)} copy(bf16[8,4,32,2048]{3,2,0,1:T(8,128)(2,1)} %convert_bitcast_fusion) | data formatting | bytes 8388608 | tf_op jit(solution)/shard_map/convert_element_type | solution.py:143
  99.7 0.9 constant_dynamic-slice_fusion.2
  100.8 2.9 %copy.44 = bf16[768,2,2,2,32]{4,3,2,1,0:T(2,128)(2,1)} copy(bf16[768,2,2,2,32]{0,4,3,2,1:T(8,128)(2,1)S(1)} %pad_maximum_fusion.1) | data formatting | bytes 786432 | tf_op jit(solution)/shard_map/stack | solution.py:30
  103.8 3.7 %convert_element_type.88 = bf16[1536,128]{1,0:T(8,128)(2,1)S(1)} reshape(bf16[768,2,2,2,32]{4,3,2,1,0:T(2,128)(2,1)} %copy.44) | data formatting | bytes 786432 | tf_op jit(solution)/shard_map/convert_element_type | solution.py:40
  107.5 0.9 constant_dynamic-slice_fusion.1
  108.6 0.7 subtract_convert_fusion.1
  109.4 12.7 %all_gather.6 = bf16[3072,128]{0,1:T(8,128)(2,1)S(1)} all-gather(bf16[768,128]{0,1:T(8,128)(2,1)S(1)} %bitcast.111), channel_id=1, replica_groups=mesh['ep'=4,'tp'=8] {'ep'}, dimensions={0}, use_global_device_ids=true | all-gather | bytes 983040 | tf_op jit(solution)/shard_map/all_gather | solution.py:59
  122.1 11.4 %all_gather.7 = bf16[3072,128]{1,0:T(8,128)(2,1)} all-gather(bf16[768,128]{1,0:T(8,128)(2,1)S(1)} %constant_dynamic-slice_fusion.1), channel_id=1, replica_groups=mesh['ep'=4,'tp'=8] {'ep'}, dimensions={0}, use_global_device_ids=true | all-gather | bytes 983040 | tf_op jit(solution)/shard_map/all_gather | solution.py:60
  133.5 35.9 %while.18 = (s32[]{:T(128)}, f32[1536]{0:T(1024)S(1)}, f32[1536]{0:T(1024)S(1)}, f32[1536,128]{1,0:T(8,128)S(1)}, bf16[3072,128]{0,1:T(8,128)(2,1)S(1)}, /*index...) while((s32[]{:T(128)}, f32[1536]{0:T(1024)S(1)}, ...), condition=%wide.region_5.6_spmd.clone, body=%wide.region_2.5_spmd.clone.sunk | while | flops 614014464 | bytes 35487944 | solution.py:80
  133.5 3.0 %multiply_reduce_fusion.2 = (f32[1536]{0:T(1024)S(1)}, f32[768,1536]{1,0:T(8,128)}) fusion(bf16[1536,128]{1,0:T(8,128)(2,1)S(1)} %get-tuple-element.288, bf16[3072,128]{0,1:T(8,128)(2,1)S(1)} %get-tuple-element.287, s32[]{:T(128)S(6)} %select_n.72), kind=kOutput, calls=%fused_computation.1.clone.1 | convolution fusion | flops 304347648 | bytes 5314564 | tf_op jit(solution)/shard_map/while/body/eval_jaxpr/qd,sd->qs/dot_general | solution.py:68
  136.5 3.3 %fusion.88 = f32[1536]{0:T(1024)S(1)} fusion(f32[768,1536]{1,0:T(8,128)} %get-tuple-element.258, f32[1536]{0:T(1024)S(1)} %select_maximum_fusion.2), kind=kLoop, calls=%fused_computation.3.clone.1 | loop fusion | flops 3537408 | bytes 4730880 | tf_op jit(solution)/shard_map/while/body/eval_jaxpr/reduce_sum | solution.py:74
  139.9 0.5 copy-done.1
  140.4 2.1 convolution_add_fusion.2
  142.6 3.0 %multiply_reduce_fusion.2 = (f32[1536]{0:T(1024)S(1)}, f32[768,1536]{1,0:T(8,128)}) fusion(bf16[1536,128]{1,0:T(8,128)(2,1)S(1)} %get-tuple-element.288, bf16[3072,128]{0,1:T(8,128)(2,1)S(1)} %get-tuple-element.287, s32[]{:T(128)S(6)} %select_n.72), kind=kOutput, calls=%fused_computation.1.clone.1 | convolution fusion | flops 304347648 | bytes 5314564 | tf_op jit(solution)/shard_map/while/body/eval_jaxpr/qd,sd->qs/dot_general | solution.py:68
  145.6 3.3 %fusion.88 = f32[1536]{0:T(1024)S(1)} fusion(f32[768,1536]{1,0:T(8,128)} %get-tuple-element.258, f32[1536]{0:T(1024)S(1)} %select_maximum_fusion.2), kind=kLoop, calls=%fused_computation.3.clone.1 | loop fusion | flops 3537408 | bytes 4730880 | tf_op jit(solution)/shard_map/while/body/eval_jaxpr/reduce_sum | solution.py:74
  148.9 0.5 copy-done.1
  149.4 2.1 convolution_add_fusion.2
  151.6 3.0 %multiply_reduce_fusion.2 = (f32[1536]{0:T(1024)S(1)}, f32[768,1536]{1,0:T(8,128)}) fusion(bf16[1536,128]{1,0:T(8,128)(2,1)S(1)} %get-tuple-element.288, bf16[3072,128]{0,1:T(8,128)(2,1)S(1)} %get-tuple-element.287, s32[]{:T(128)S(6)} %select_n.72), kind=kOutput, calls=%fused_computation.1.clone.1 | convolution fusion | flops 304347648 | bytes 5314564 | tf_op jit(solution)/shard_map/while/body/eval_jaxpr/qd,sd->qs/dot_general | solution.py:68
  154.6 3.3 %fusion.88 = f32[1536]{0:T(1024)S(1)} fusion(f32[768,1536]{1,0:T(8,128)} %get-tuple-element.258, f32[1536]{0:T(1024)S(1)} %select_maximum_fusion.2), kind=kLoop, calls=%fused_computation.3.clone.1 | loop fusion | flops 3537408 | bytes 4730880 | tf_op jit(solution)/shard_map/while/body/eval_jaxpr/reduce_sum | solution.py:74
  157.9 0.4 copy-done.1
  158.4 2.1 convolution_add_fusion.2
  160.5 3.0 %multiply_reduce_fusion.2 = (f32[1536]{0:T(1024)S(1)}, f32[768,1536]{1,0:T(8,128)}) fusion(bf16[1536,128]{1,0:T(8,128)(2,1)S(1)} %get-tuple-element.288, bf16[3072,128]{0,1:T(8,128)(2,1)S(1)} %get-tuple-element.287, s32[]{:T(128)S(6)} %select_n.72), kind=kOutput, calls=%fused_computation.1.clone.1 | convolution fusion | flops 304347648 | bytes 5314564 | tf_op jit(solution)/shard_map/while/body/eval_jaxpr/qd,sd->qs/dot_general | solution.py:68
  163.5 3.3 %fusion.88 = f32[1536]{0:T(1024)S(1)} fusion(f32[768,1536]{1,0:T(8,128)} %get-tuple-element.258, f32[1536]{0:T(1024)S(1)} %select_maximum_fusion.2), kind=kLoop, calls=%fused_computation.3.clone.1 | loop fusion | flops 3537408 | bytes 4730880 | tf_op jit(solution)/shard_map/while/body/eval_jaxpr/reduce_sum | solution.py:74
  166.8 0.4 copy-done.1
  167.3 2.1 convolution_add_fusion.2
  169.5 0.3 divide_convert_fusion
  169.9 2.7 %convolution_convert_fusion = bf16[768,2048]{1,0:T(8,128)(2,1)} fusion(bf16[768,256]{1,0:T(8,128)(2,1)S(1)} %reshape.434, bf16[256,2048]{1,0:T(8,128)(2,1)S(1)} %copy-done), kind=kOutput, calls=%fused_computation.33 | convolution fusion | flops 806879232 | bytes 4587520 | tf_op jit(solution)/shard_map/dot_general | solution.py:83
  172.6 0.2 iota_compare_fusion
  172.8 1.9 copy.52
  174.7 3.5 %all-to-all-start.1 = ((bf16[4,4,8,2048]{3,2,0,1:T(8,128)(2,1)}), bf16[4,4,8,2048]{3,2,0,1:T(8,128)(2,1)S(1)}, u32[]{:S(2)}, u32[]{:S(2)}) async-start(bf16[4,4,8,2048]{3,2,0,1:T(8,128)(2,1)} %copy.52), calls=%async_computation.3 | async-start | bytes 1048576 | tf_op jit(solution)/shard_map/all_to_all | solution.py:145
  178.5 0.2 fusion.51
  178.7 6.0 %all-to-all-done.1 = bf16[4,4,8,2048]{3,2,0,1:T(8,128)(2,1)S(1)} async-done(((bf16[4,4,8,2048]{3,2,0,1:T(8,128)(2,1)}), bf16[4,4,8,2048]{3,2,0,1:T(8,128)(2,1)S(1)}, u32[]{:S(2)}, u32[]{:S(2)}) %all-to-all-start.1) | async-done | bytes 524320 | tf_op jit(solution)/shard_map/all_to_all | solution.py:145
  184.7 1.0 convolution_convert_fusion.1
  185.7 28.1 %reduce-scatter.3.cloned.1.call-done = bf16[96,2048]{1,0:T(8,128)(2,1)} async-done(((bf16[768,2048]{1,0:T(8,128)(2,1)}), bf16[96,2048]{1,0:T(8,128)(2,1)}) %reduce-scatter.3.cloned.1.call-update) | async-done | bytes 393232 | tf_op jit(solution)/shard_map/reduce_scatter | solution.py:82
  (60 shorter events, 1.8 us)
Async XLA Ops:
  7.2 162.7 %copy-start = (bf16[256,2048]{1,0:T(8,128)(2,1)S(1)}, bf16[256,2048]{1,0:T(8,128)(2,1)}, u32[]{:S(2)}) copy-start(bf16[256,2048]{1,0:T(8,128)(2,1)} %param.20) | copy-start | bytes 3145732
  18.4 5.3 %copy-start.2 = (bf16[768,256]{1,0:T(8,128)(2,1)S(1)}, bf16[768,256]{1,0:T(8,128)(2,1)}, u32[]{:S(2)}) copy-start(bf16[768,256]{1,0:T(8,128)(2,1)} %param.15) | copy-start | bytes 1179652
  18.4 5.5 %copy-start.4 = (f32[128]{0:T(128)S(1)}, f32[128]{0:T(128)}, u32[]{:S(2)}) copy-start(f32[128]{0:T(128)} %param.18) | copy-start | bytes 1540
  18.4 53.9 %all-to-all-start = ((bf16[4,8,4,8,2048]{4,3,2,1,0:T(8,128)(2,1)}), bf16[4,8,4,8,2048]{4,3,2,1,0:T(8,128)(2,1)}, u32[]{:S(2)}, u32[]{:S(2)}) async-start(bf16[4,8,4,8,2048]{4,3,2,1,0:T(8,128)(2,1)} %pad_maximum_fusion), calls=%async_computation.1 | async-start | bytes 8388608 | tf_op jit(solution)/shard_map/all_to_all | solution.py:126
  23.7 149.1 %reduce-scatter.5.cloned.1.call-start = ((), (), s32[]{:S(2)}) async-start(), calls=%async_computation.5 | async-start | bytes 4718592 | tf_op jit(solution)/shard_map/reduce_scatter | solution.py:142
  99.6 8.9 %copy-start.5 = (f32[128]{0:T(128)S(1)}, f32[128]{0:T(128)}, u32[]{:S(2)}) copy-start(f32[128]{0:T(128)} %param.19) | copy-start | bytes 1540
  99.7 114.2 %reduce-scatter.3.cloned.1.call-start = ((), (), s32[]{:S(2)}) async-start(), calls=%async_computation.4 | async-start | bytes 3538944 | tf_op jit(solution)/shard_map/reduce_scatter | solution.py:82
  136.5 3.9 %copy-start.1 = (f32[768,1536]{1,0:T(8,128)S(1)}, f32[768,1536]{1,0:T(8,128)}, u32[]{:S(2)}) copy-start(f32[768,1536]{1,0:T(8,128)} %get-tuple-element.258) | copy-start | bytes 14155780 | tf_op jit(solution)/shard_map/while
  145.6 3.9 %copy-start.1 = (f32[768,1536]{1,0:T(8,128)S(1)}, f32[768,1536]{1,0:T(8,128)}, u32[]{:S(2)}) copy-start(f32[768,1536]{1,0:T(8,128)} %get-tuple-element.258) | copy-start | bytes 14155780 | tf_op jit(solution)/shard_map/while
  154.6 3.8 %copy-start.1 = (f32[768,1536]{1,0:T(8,128)S(1)}, f32[768,1536]{1,0:T(8,128)}, u32[]{:S(2)}) copy-start(f32[768,1536]{1,0:T(8,128)} %get-tuple-element.258) | copy-start | bytes 14155780 | tf_op jit(solution)/shard_map/while
  163.5 3.8 %copy-start.1 = (f32[768,1536]{1,0:T(8,128)S(1)}, f32[768,1536]{1,0:T(8,128)}, u32[]{:S(2)}) copy-start(f32[768,1536]{1,0:T(8,128)} %get-tuple-element.258) | copy-start | bytes 14155780 | tf_op jit(solution)/shard_map/while
  169.9 2.7 %copy-start.3 = (f32[384,2]{0,1:T(2,128)S(1)}, f32[384,2]{0,1:T(2,128)}, u32[]{:S(2)}) copy-start(f32[384,2]{0,1:T(2,128)} %param.24) | copy-start | bytes 9220
  174.7 10.0 %all-to-all-start.1 = ((bf16[4,4,8,2048]{3,2,0,1:T(8,128)(2,1)}), bf16[4,4,8,2048]{3,2,0,1:T(8,128)(2,1)S(1)}, u32[]{:S(2)}, u32[]{:S(2)}) async-start(bf16[4,4,8,2048]{3,2,0,1:T(8,128)(2,1)} %copy.52), calls=%async_computation.3 | async-start | bytes 1048576 | tf_op jit(solution)/shard_map/all_to_all | solution.py:145
Sparse Core Ops, SparseCore 0:
  99.8 50.3 reduce-scatter.4
  172.7 41.1 reduce-scatter.2
